TPU v7x, 128 devices: a whole 4x4x4 slice. The times are simulated.
128 devices in a mesh: ep: 64 (over z, y, x), tp: 2 (over core).
Axes of the slice: x: 4, y: 4, z: 4, core: 2. Of those that a mesh axis runs over, the one named last changes fastest.
Arguments:
- tokens: bfloat16 [1024, 2048], P('ep'), may hold values from -6 to 6
- mix_gain: float32 [2048], replicated, may hold values from 0.1 to 1.9
- w_query: bfloat16 [2048, 1024], P(None, 'tp'), may hold values from -0.125 to 0.125
- w_forget: bfloat16 [2048, 1024], P(None, 'tp'), may hold values from -0.125 to 0.125
- w_input: bfloat16 [2048, 1024], P(None, 'tp'), may hold values from -0.125 to 0.125
- w_outgate: bfloat16 [2048, 1024], P(None, 'tp'), may hold values from -0.125 to 0.125
- decay_floor: float32 [1024], P('tp'), may hold values from 0 to 0.9
- head_gain: float32 [128], replicated, may hold values from 0.1 to 1.9
- prev_state: float32 [1024, 8, 128, 128], P('ep', 'tp'), may hold values from -4 to 4
- w_output: bfloat16 [1024, 2048], P('tp'), may hold values from -0.1875 to 0.1875
- moe_gain: float32 [2048], replicated, may hold values from 0.1 to 1.9
- route_ids: int32 [1024, 2], P('ep'), may hold values from 0 to 31, all different within a row; in each aligned block of 16 rows (0 to 15, 16 to 31, ...) at most 8 rows name the same one
- route_logits: float32 [1024, 2], P('ep'), may hold values from -6 to 6
- w_exp_gate: bfloat16 [64, 2048, 1536], P('ep', None, 'tp'), may hold values from -0.125 to 0.125
- w_exp_up: bfloat16 [64, 2048, 1536], P('ep', None, 'tp'), may hold values from -0.125 to 0.125
- w_exp_down: bfloat16 [64, 1536, 2048], P('ep', 'tp'), may hold values from -0.109375 to 0.109375
Outputs:
- layer_out: bfloat16 [1024, 2048], P('ep')
- new_state: float32 [1024, 8, 128, 128], P('ep', 'tp')
Inputs may be any that keep to these rules, and one draw needn't show every extreme that they name: `route_ids`: each row names 2 different experts; within the rows of one device no expert is named more than 8 times, and in every draw some expert is named exactly 8 times in some device's rows.
All inputs are finite; a program needn't handle non-finite values.
Results may differ from a plain program's by a relative error of at most 0.014.
Values may be sent and summed in bfloat16 or wider, within the bound.
A program may use at most 128 MiB of HBM per device.

v0:
```python
import jax
import jax.numpy as jnp
from jax import lax
from jax.sharding import PartitionSpec as P

TOP_K = 2


epsilon = 1e-06


def total_of_pieces(shard, axis):
    return lax.all_gather(shard, axis).astype(jnp.float32).sum(0)


def in_blocks(shard, dim, peers):
    before, after = (shard.shape[:dim], shard.shape[dim + 1 :])
    return jnp.moveaxis(shard.reshape(*before, peers, -1, *after), dim, 0)


def summed_on_arrival(shard, axis, dim):
    pieces = in_blocks(shard, dim, lax.axis_size(axis))
    arrived = lax.all_to_all(pieces, axis, split_axis=0, concat_axis=0, tiled=True)
    return arrived.astype(jnp.float32).sum(axis=0)


def from_everyone(shard, axis):
    peers = lax.axis_size(axis)
    return lax.all_to_all(
        jnp.broadcast_to(shard[None], (peers, *shard.shape)), axis, 0, 0, tiled=True
    )


def joined_along(pieces, dim):
    shape = list(pieces.shape[1:])
    shape[dim] *= pieces.shape[0]
    return jnp.moveaxis(pieces, 0, dim).reshape(shape)


def collect(shard, axis, dim):
    pieces = from_everyone(shard, axis)
    return joined_along(pieces, dim)


def rms_scale(values, gains):
    return values * lax.rsqrt(jnp.mean(values * values, axis=-1, keepdims=True) + epsilon) * gains


def on_device(
    tokens,
    mix_gain,
    w_query,
    w_forget,
    w_input,
    w_outgate,
    decay_floor,
    head_gain,
    prev_state,
    w_output,
    moe_gain,
    route_ids,
    route_logits,
    w_exp_gate,
    w_exp_up,
    w_exp_down,
):
    seq_dev = tokens.shape[0]
    ep_size = lax.axis_size("ep")
    residual = tokens.astype(jnp.float32)
    normed = rms_scale(residual, mix_gain).astype(jnp.bfloat16)
    heads_dev = prev_state.shape[1]
    head_dim = prev_state.shape[2]
    head_width = heads_dev * head_dim
    query_part = jnp.dot(normed, w_query, preferred_element_type=jnp.float32).reshape(
        seq_dev, heads_dev, head_dim
    )
    forget_pre = jnp.dot(normed, w_forget, preferred_element_type=jnp.float32).reshape(
        seq_dev, heads_dev, head_dim
    )
    value_part = jnp.dot(normed, w_input, preferred_element_type=jnp.float32).reshape(
        seq_dev, heads_dev, head_dim
    )
    outgate_pre = jnp.dot(normed, w_outgate, preferred_element_type=jnp.float32).reshape(
        seq_dev, heads_dev, head_dim
    )
    floor_rate = decay_floor.reshape(heads_dev, head_dim)
    forget = floor_rate + (1.0 - floor_rate) * jax.nn.sigmoid(forget_pre)
    key_part = (1.0 - floor_rate) * jax.nn.sigmoid(-forget_pre)
    new_state = forget[..., None] * prev_state + key_part[..., None] * value_part[:, :, None, :]
    readout = jnp.sum(query_part[..., None] * new_state, axis=2)
    gated = (
        (rms_scale(readout, head_gain) * jax.nn.silu(outgate_pre))
        .reshape(seq_dev, head_width)
        .astype(jnp.bfloat16)
    )
    mixed_out = total_of_pieces(
        jnp.dot(gated, w_output, preferred_element_type=jnp.float32).astype(jnp.bfloat16), "tp"
    ).astype(jnp.float32)
    middle = (residual + mixed_out).astype(jnp.bfloat16)
    normed_two = rms_scale(middle.astype(jnp.float32), moe_gain).astype(jnp.bfloat16)
    experts = ep_size // 2
    capacity = min(seq_dev, max(2, 8 * seq_dev * TOP_K // experts))
    slot_total = ep_size * capacity
    pair_expert = route_ids.reshape(-1)
    onehot = (pair_expert[:, None] == jnp.arange(experts, dtype=jnp.int32)[None, :]).astype(
        jnp.int32
    )
    slot_rank = jnp.sum((jnp.cumsum(onehot, axis=0) - onehot) * onehot, axis=1)
    slot_ids = jnp.arange(slot_total, dtype=jnp.int32)
    slot_expert = slot_ids // capacity // 2
    slot_order = slot_ids % capacity
    matches = (slot_expert[:, None] == pair_expert[None, :]) & (
        slot_order[:, None] == slot_rank[None, :]
    )
    match_tok = jnp.any(matches.reshape(slot_total, seq_dev, TOP_K), axis=2)
    outgoing = (
        jnp.dot(match_tok.astype(jnp.bfloat16), normed_two, preferred_element_type=jnp.float32)
        .astype(jnp.bfloat16)
        .reshape(ep_size, capacity, -1)
    )
    arrived = lax.all_to_all(outgoing, "ep", split_axis=0, concat_axis=0, tiled=True)
    per_source = arrived.shape[1]
    slot_rows = arrived.reshape(ep_size * per_source, arrived.shape[2])
    gate_pre = jnp.dot(slot_rows, w_exp_gate[0], preferred_element_type=jnp.float32)
    up_pre = jnp.dot(slot_rows, w_exp_up[0], preferred_element_type=jnp.float32)
    activated = (jax.nn.silu(gate_pre) * up_pre).astype(jnp.bfloat16)
    partial_down = jnp.dot(activated, w_exp_down[0], preferred_element_type=jnp.float32)
    share = summed_on_arrival(partial_down.astype(jnp.bfloat16), "tp", 1)
    answer = share.astype(jnp.bfloat16).reshape(ep_size, per_source, -1)
    returned = lax.all_to_all(answer, "ep", split_axis=0, concat_axis=0, tiled=True)
    returned = collect(returned, "tp", 2)
    weights = jax.nn.sigmoid(route_logits - jnp.flip(route_logits, axis=1)).reshape(-1)
    combine = jnp.sum(
        (matches.astype(jnp.float32) * weights[None, :]).reshape(slot_total, seq_dev, TOP_K), axis=2
    ).T
    expert_sum = jnp.dot(combine, returned.reshape(slot_total, -1).astype(jnp.float32))
    layer_out = (middle.astype(jnp.float32) + expert_sum).astype(jnp.bfloat16)
    return (layer_out, new_state)


def solution(mesh):
    placed = (
        P("ep", None),
        P(),
        P(None, "tp"),
        P(None, "tp"),
        P(None, "tp"),
        P(None, "tp"),
        P("tp"),
        P(),
        P("ep", "tp", None, None),
        P("tp", None),
        P(),
        P("ep", None),
        P("ep", None),
        P("ep", None, "tp"),
        P("ep", None, "tp"),
        P("ep", "tp", None),
    )
    return jax.shard_map(
        on_device,
        mesh=mesh,
        in_specs=placed,
        out_specs=(P("ep", None), P("ep", "tp", None, None)),
        check_vma=False,
    )
```

profile of v0, /device:TPU:1, one launch (start us, length us, event | category | flops | bytes accessed | tf_op | source)
XLA Modules:
  0.0 125.9 jit_solution(11129159292883252952)
XLA Ops:
  0.6 0.0 copy-start
  0.6 0.0 copy-start.1
  0.7 0.0 copy-start.3
  0.7 0.0 copy-start.6
  0.7 1.1 fusion.22
  1.8 2.1 %add_divide_fusion.1 = (f32[16,512]{1,0:T(8,128)S(1)}, f32[16,512]{1,0:T(8,128)S(1)}) fusion(bf16[2048,512]{1,0:T(8,128)(2,1)} %param.19, bf16[16,2048]{1,0:T(8,128)(2,1)} %param.16, f32[2048]{0:T(1024)} %param.17, f32[16]{0:T(128)S(1)} %add_rsqrt_fusion.2), kind=kOutput, calls=%fused_computation.44 | convolution fusion | flops 33726464 | bytes 2236480 | tf_op jit(solution)/shard_map/dot_general | solution.py:77
  4.0 0.0 copy-done.6
  4.0 0.0 copy-done.1
  4.0 0.0 copy-done.3
  4.0 2.0 %fusion.59 = f32[16,512]{1,0:T(8,128)S(1)} fusion(bf16[2048,512]{1,0:T(8,128)(2,1)} %param.18, bf16[16,2048]{1,0:T(8,128)(2,1)S(1)} %copy-done.1, f32[2048]{0:T(1024)S(1)} %copy-done.3, f32[16]{0:T(128)S(1)} %add_rsqrt_fusion.2), kind=kOutput, calls=%fused_computation.83 | convolution fusion | flops 33685504 | bytes 2203712 | tf_op jit(solution)/shard_map/dot_general | solution.py:74
  6.0 2.0 %fusion.55 = f32[16,512]{1,0:T(8,128)S(1)} fusion(bf16[2048,512]{1,0:T(8,128)(2,1)} %param.20, bf16[16,2048]{1,0:T(8,128)(2,1)S(1)} %copy-done.1, f32[2048]{0:T(1024)S(1)} %copy-done.3, f32[16]{0:T(128)S(1)} %add_rsqrt_fusion.2), kind=kOutput, calls=%fused_computation.81 | convolution fusion | flops 33685504 | bytes 2203712 | tf_op jit(solution)/shard_map/dot_general | solution.py:80
  8.1 0.0 copy-start.8
  8.1 8.1 %multiply_reduce_fusion = (f32[16,4,128]{2,1,0:T(4,128)S(1)}, f32[16,4,128,128]{3,2,1,0:T(8,128)}) fusion(f32[16,4,128]{2,1,0:T(4,128)S(1)} %mul.153, f32[16,4,128]{2,1,0:T(4,128)S(1)} %mul.161, f32[16,4,128]{2,1,0:T(4,128)S(1)} %bitcast.75, f32[16,4,128,128]{3,2,1,0:T(8,128)} %param.24, f32[16,4,128]{2,1,0:T(4,128)S(1)} %bitcast.74), kind=kLoop, calls=%fused_computation | loop fusion | flops 5234688 | bytes 8552448 | tf_op jit(solution)/shard_map/reduce_sum | solution.py:90
  16.2 0.1 multiply_reduce_fusion.1
  16.4 0.1 broadcast_multiply_fusion
  16.4 0.0 copy-done.8
  16.5 0.0 copy-start.4
  16.5 0.0 copy-start.5
  16.5 3.0 %convolution_convert_fusion.1 = bf16[16,2048]{1,0:T(8,128)(2,1)S(1)} fusion(bf16[512,2048]{1,0:T(8,128)(2,1)} %param.25, f32[2,8,4,128]{3,2,1,0:T(4,128)S(1)} %bitcast.76, f32[512]{0:T(512)S(1)} %broadcast_bitcast_fusion, bf16[2048,512]{1,0:T(8,128)(2,1)} %param.21, bf16[16,2048]{1,0:T(8,128)(2,1)S(1)} %copy-done.1, f32[2048]{0:T(1024)S(1)} %copy-done.3, ...), kind=kOutput, calls=%fused_computation.13 | convolution fusion | flops 67330048 | bytes 4368448 | tf_op jit(solution)/shard_map/dot_general | solution.py:97
  19.5 2.9 %all-gather = bf16[32,2048]{1,0:T(8,128)(2,1)S(1)} all-gather(bf16[16,2048]{1,0:T(8,128)(2,1)S(1)} %convolution_convert_fusion.1), channel_id=2, replica_groups=mesh['ep'=64,'tp'=2] {'tp'}, dimensions={0}, use_global_device_ids=true | all-gather | bytes 196608 | tf_op jit(solution)/shard_map/all_gather | solution.py:13
  22.5 0.1 fusion.26
  22.6 0.0 copy-done.4
  22.6 0.1 copy.29
  22.7 0.1 eq.53
  22.8 0.1 fusion.36
  22.9 0.1 reduce_window_sum.11
  22.9 0.2 select_reduce_fusion.1
  23.1 0.1 eq.57
  23.2 0.1 copy.30
  23.3 0.1 fusion.32
  23.4 0.0 copy-done.5
  23.4 0.8 fusion.9
  24.2 0.0 copy-start.9
  24.2 40.3 %all_to_all.20 = bf16[64,8,2048]{2,1,0:T(8,128)(2,1)S(1)} all-to-all(bf16[64,8,2048]{2,1,0:T(8,128)(2,1)S(1)} %fusion.9), channel_id=1, replica_groups=mesh['ep'=64,'tp'=2] {'ep'}, dimensions={0} | all-to-all | bytes 4194304 | tf_op jit(solution)/shard_map/all_to_all | solution.py:121
  64.5 0.0 copy-start.2
  64.5 1.3 %copy-done.2 = bf16[64,8,2048]{2,1,0:T(8,128)(2,1)} copy-done((bf16[64,8,2048]{2,1,0:T(8,128)(2,1)}, bf16[64,8,2048]{2,1,0:T(8,128)(2,1)S(1)}, u32[]{:S(2)}) %copy-start.2) | copy-done | bytes 2097176
  65.8 0.0 copy-done.9
  65.8 3.0 %fusion.4 = f32[512,768]{1,0:T(8,128)} fusion(bf16[1,2048,768]{2,1,0:T(8,128)(2,1)S(1)} %copy-done.9, bf16[64,8,2048]{2,1,0:T(8,128)(2,1)S(1)} %all_to_all.20), kind=kOutput, calls=%fused_computation.6 | convolution fusion | flops 1610612736 | bytes 6815744 | tf_op jit(solution)/shard_map/dot_general | solution.py:124
  68.8 0.0 copy-done
  68.8 8.2 %fusion.6 = bf16[512,2048]{1,0:T(8,128)(2,1)} fusion(bf16[1,768,2048]{2,1,0:T(8,128)(2,1)S(1)} %copy-done, f32[512,768]{1,0:T(8,128)} %fusion.4, bf16[1,2048,768]{2,1,0:T(8,128)(2,1)} %param.30, bf16[64,8,2048]{2,1,0:T(8,128)(2,1)} %copy-done.2), kind=kOutput, calls=%fused_computation.8 | convolution fusion | flops 3224633344 | bytes 12058624 | tf_op jit(solution)/shard_map/dot_general | solution.py:127
  77.0 1.8 %copy.40 = bf16[64,2,8,1024]{3,2,0,1:T(8,128)(2,1)S(1)} copy(bf16[64,2,8,1024]{3,2,1,0:T(8,128)(2,1)} %bitcast.72) | data formatting | bytes 4194304 | tf_op jit(solution)/shard_map/reshape | solution.py:18
  78.8 8.0 %all_to_all.21 = bf16[2,512,1024]{2,1,0:T(8,128)(2,1)} all-to-all(bf16[2,512,1024]{2,1,0:T(8,128)(2,1)S(1)} %bitcast.69), channel_id=1, replica_groups=mesh['ep'=64,'tp'=2] {'tp'}, dimensions={0} | all-to-all | bytes 4194304 | tf_op jit(solution)/shard_map/all_to_all | solution.py:23
  86.8 0.0 copy-start.7
  86.8 3.3 %reduce_sum.82 = bf16[512,1024]{1,0:T(8,128)(2,1)} reduce(bf16[2,512,1024]{2,1,0:T(8,128)(2,1)} %all_to_all.21, bf16[]{:T(256)} %constant.69.clone.1), dimensions={0}, to_apply=%region_9.10 | reduce | flops 524288 | bytes 3145730 | tf_op jit(solution)/shard_map/reduce_sum | solution.py:24
  90.1 5.7 %all-to-all-start.2 = ((bf16[64,8,1024]{2,1,0:T(8,128)(2,1)}), bf16[64,8,1024]{2,1,0:T(8,128)(2,1)}, u32[]{:S(2)}, u32[]{:S(2)}) async-start(bf16[64,8,1024]{2,1,0:T(8,128)(2,1)} %bitcast.71), calls=%async_computation.2 | async-start | bytes 2097152 | tf_op jit(solution)/shard_map/all_to_all | solution.py:130
  95.8 0.0 copy-done.7
  95.9 0.1 select_reduce_fusion
  96.0 17.8 %all-to-all-done.2 = bf16[64,8,1024]{2,1,0:T(8,128)(2,1)} async-done(((bf16[64,8,1024]{2,1,0:T(8,128)(2,1)}), bf16[64,8,1024]{2,1,0:T(8,128)(2,1)}, u32[]{:S(2)}, u32[]{:S(2)}) %all-to-all-start.2) | async-done | bytes 1048608 | tf_op jit(solution)/shard_map/all_to_all | solution.py:130
  113.7 1.5 %broadcast_in_dim.2 = bf16[2,64,8,1024]{3,2,1,0:T(8,128)(2,1)S(1)} broadcast(bf16[64,8,1024]{2,1,0:T(8,128)(2,1)} %all-to-all-done.2), dimensions={1,2,3} | broadcast | bytes 3145728 | tf_op jit(solution)/shard_map/broadcast_in_dim | solution.py:30
  115.2 6.9 %all_to_all.22 = bf16[2,64,8,1024]{3,2,1,0:T(8,128)(2,1)S(1)} all-to-all(bf16[2,64,8,1024]{3,2,1,0:T(8,128)(2,1)S(1)} %broadcast_in_dim.2), channel_id=1, replica_groups=mesh['ep'=64,'tp'=2] {'tp'}, dimensions={0} | all-to-all | bytes 4194304 | tf_op jit(solution)/shard_map/all_to_all | solution.py:29
  122.1 2.2 %copy.41 = bf16[64,8,2,1024]{3,2,1,0:T(2,128)(2,1)S(1)} copy(bf16[64,8,2,1024]{3,1,0,2:T(8,128)(2,1)S(1)} %bitcast.70) | data formatting | bytes 4194304 | tf_op jit(solution)/shard_map/transpose | solution.py:37
  124.2 0.6 copy.35
  124.8 1.0 fusion.10
  (16 shorter events, 0.2 us)
Async XLA Ops:
  0.6 68.2 %copy-start = (bf16[1,768,2048]{2,1,0:T(8,128)(2,1)S(1)}, bf16[1,768,2048]{2,1,0:T(8,128)(2,1)}, u32[]{:S(2)}) copy-start(bf16[1,768,2048]{2,1,0:T(8,128)(2,1)} %param.31) | copy-start | bytes 9437188
  0.6 3.3 %copy-start.1 = (bf16[16,2048]{1,0:T(8,128)(2,1)S(1)}, bf16[16,2048]{1,0:T(8,128)(2,1)}, u32[]{:S(2)}) copy-start(bf16[16,2048]{1,0:T(8,128)(2,1)} %param.16) | copy-start | bytes 196612
  0.7 3.3 %copy-start.3 = (f32[2048]{0:T(1024)S(1)}, f32[2048]{0:T(1024)}, u32[]{:S(2)}) copy-start(f32[2048]{0:T(1024)} %param.17) | copy-start | bytes 24580
  0.7 3.3 %copy-start.6 = (f32[512]{0:T(512)S(1)}, f32[512]{0:T(512)}, u32[]{:S(2)}) copy-start(f32[512]{0:T(512)} %param.22) | copy-start | bytes 6148
  8.1 8.3 %copy-start.8 = (f32[128]{0:T(128)S(1)}, f32[128]{0:T(128)}, u32[]{:S(2)}) copy-start(f32[128]{0:T(128)} %param.23) | copy-start | bytes 1540
  16.5 6.1 %copy-start.4 = (s32[16,2]{0,1:T(2,128)S(1)}, s32[16,2]{0,1:T(2,128)}, u32[]{:S(2)}) copy-start(s32[16,2]{0,1:T(2,128)} %param.27) | copy-start | bytes 388
  16.5 6.9 %copy-start.5 = (f32[2048]{0:T(1024)S(1)}, f32[2048]{0:T(1024)}, u32[]{:S(2)}) copy-start(f32[2048]{0:T(1024)} %param.26) | copy-start | bytes 24580
  24.2 41.7 %copy-start.9 = (bf16[1,2048,768]{2,1,0:T(8,128)(2,1)S(1)}, bf16[1,2048,768]{2,1,0:T(8,128)(2,1)}, u32[]{:S(2)}) copy-start(bf16[1,2048,768]{2,1,0:T(8,128)(2,1)} %param.29) | copy-start | bytes 9437188
  64.5 1.4 %copy-start.2 = (bf16[64,8,2048]{2,1,0:T(8,128)(2,1)}, bf16[64,8,2048]{2,1,0:T(8,128)(2,1)S(1)}, u32[]{:S(2)}) copy-start(bf16[64,8,2048]{2,1,0:T(8,128)(2,1)S(1)} %all_to_all.20) | copy-start | bytes 6291460
  86.8 9.0 %copy-start.7 = (f32[16,2]{0,1:T(2,128)S(1)}, f32[16,2]{0,1:T(2,128)}, u32[]{:S(2)}) copy-start(f32[16,2]{0,1:T(2,128)} %param.28) | copy-start | bytes 388
  90.1 23.6 %all-to-all-start.2 = ((bf16[64,8,1024]{2,1,0:T(8,128)(2,1)}), bf16[64,8,1024]{2,1,0:T(8,128)(2,1)}, u32[]{:S(2)}, u32[]{:S(2)}) async-start(bf16[64,8,1024]{2,1,0:T(8,128)(2,1)} %bitcast.71), calls=%async_computation.2 | async-start | bytes 2097152 | tf_op jit(solution)/shard_map/all_to_all | solution.py:130
where the time goes:
time: 127 us; the launch traced here: 126 us
  blocking collectives  58.1 us (46%)
  matrix products  22.1 us (17%)
  waiting for transfers between devices  17.8 us (14%)
  other arithmetic  13.4 us (11%)
  local copies, waits for them, and re-layouts  7.83 us (6%)
  starting transfers between devices  5.7 us (4%)
    all_to_all x1, blocking collectives, on_device(): lax.all_to_all(outgoing, 'ep', split_axis=0, concat_axis=0, tiled=True)  40.3 us
    all_to_all x1, waiting for transfers between devices, on_device(): lax.all_to_all(answer, 'ep', split_axis=0, concat_axis=0, tiled=True)  17.8 us
    dot_general x1, matrix products, on_device(): jnp.dot(activated, w_exp_down[0], preferred_element_type=jnp.float32)  8.23 us
    reduce_sum x1, other arithmetic, on_device(): readout = jnp.sum(query_part[..., None] * new_state, axis=2)  8.11 us
    all_to_all x1, blocking collectives, summed_on_arrival(): lax.all_to_all(pieces, axis, split_axis=0, concat_axis=0, tiled=True)  7.97 us
    all_to_all x1, blocking collectives, from_everyone(): lax.all_to_all(jnp.broadcast_to(shard[None], (peers, *shard.shape)), axis...  6.86 us
    all_to_all x1, starting transfers between devices, on_device(): lax.all_to_all(answer, 'ep', split_axis=0, concat_axis=0, tiled=True)  5.7 us
    reduce_sum x1, other arithmetic, summed_on_arrival(): return arrived.astype(jnp.float32).sum(axis=0)  3.33 us
  transfers between devices with their start and end apart: 1, of which 1 were waited for; matrix products, arithmetic and copies ran while one was open for 0% of the time, Pallas kernels for 0%

commit v1 on v0

v1 whole, which is shorter than its diff:
```python
import functools

import jax
import jax.numpy as jnp
import numpy as np
from jax import lax
from jax.experimental import pallas as pl
from jax.experimental.pallas import tpu as pltpu
from jax.sharding import PartitionSpec as P

MESH = pl.DeviceIdType.MESH
SIDE = 4
CHIPS = SIDE**3
EXPERTS = CHIPS // 2
CAP = 8
CHUNKS = 4
PER = CHIPS // CHUNKS
ROWS = PER * CAP
SEQ = 16
WIDTH = 2048
HALF = WIDTH // 2
HEADS = 4
HEAD = 128
MIX = HEADS * HEAD
HID = 768
EPS = 1e-6
BF = jnp.bfloat16
F32 = jnp.float32


def hops(offset):
    return sum(min(v, SIDE - v) for v in offset)


def offset_order():
    every = [(z, y, x) for z in range(SIDE) for y in range(SIDE) for x in range(SIDE)]
    order = []
    for k in range(CHUNKS):
        mine = [o for o in every if sum(o) % SIDE == k]
        order += sorted(mine, key=lambda o: (o != (0, 0, 0), -hops(o), o))
    return order


OFFSETS = offset_order()


def slot_table():
    packed = [z * 16 + y * 4 + x for z, y, x in OFFSETS]
    return np.repeat(np.array(packed, np.int32), CAP)[None, :]


def rms(values, gains):
    return values * lax.rsqrt(jnp.mean(values * values, axis=-1, keepdims=True) + EPS) * gains


def layer_kernel(
    tokens,
    mix_gain,
    floor,
    head_gain,
    moe_gain,
    ids,
    ids_t,
    logits,
    table,
    w_query,
    w_forget,
    w_input,
    w_outgate,
    prev,
    w_output,
    w_gate,
    w_up,
    w_down,
    out,
    forget_t,
    value_out,
    wq_v,
    wf_v,
    wi_v,
    wg_v,
    prev_v,
    wo_v,
    eg_v,
    eu_v,
    ed_v,
    readout_v,
    part_own,
    part_sib,
    n2_v,
    middle_v,
    outgoing,
    inbox,
    down_send,
    down_recv,
    ret_out,
    ret_in,
    final,
    load_sem,
    prev_sem,
    expert_sem,
    pair_sem,
    disp_send,
    disp_recv,
    fwd_send,
    fwd_recv,
    down_sems,
    down_recv_sems,
    ret_send,
    ret_recv,
):
    me = lax.axis_index("ep")
    c = lax.axis_index("tp")
    other = 1 - c
    z, y, x = lax.div(me, 16), lax.rem(lax.div(me, 4), 4), lax.rem(me, 4)
    z_to = [lax.rem(z + d, 4) * 16 for d in range(4)]
    y_to = [lax.rem(y + d, 4) * 4 for d in range(4)]
    x_to = [lax.rem(x + d, 4) for d in range(4)]

    def ahead(o):
        return z_to[o[0]] + y_to[o[1]] + x_to[o[2]]

    def behind(o):
        return z_to[-o[0] % 4] + y_to[-o[1] % 4] + x_to[-o[2] % 4]

    def to_sibling(src, dst, send, recv):
        return pltpu.make_async_remote_copy(
            src_ref=src, dst_ref=dst, send_sem=send, recv_sem=recv, device_id={"tp": other}, device_id_type=MESH
        )

    barrier = pltpu.get_barrier_semaphore()
    pl.semaphore_signal(barrier, inc=1, device_id={"tp": other}, device_id_type=MESH)
    for o in OFFSETS[1:]:
        pl.semaphore_signal(barrier, inc=1, device_id={"ep": ahead(o)}, device_id_type=MESH)

    loads = [
        pltpu.make_async_copy(src, dst, load_sem.at[i])
        for i, (src, dst) in enumerate(
            ((w_forget, wf_v), (w_query, wq_v), (w_input, wi_v), (w_outgate, wg_v), (w_output, wo_v))
        )
    ]
    prev_loads = [
        pltpu.make_async_copy(prev.at[pl.ds(4 * i, 4)], prev_v.at[pl.ds(4 * i, 4)], prev_sem.at[i]) for i in range(4)
    ]
    loads[0].start()
    loads[1].start()
    loads[2].start()
    for copy in prev_loads:
        copy.start()
    loads[3].start()
    loads[4].start()

    ids_col = [ids[:, k : k + 1] for k in range(2)]
    ids_row = [ids_t[k : k + 1, :] for k in range(2)]
    rows16 = lax.broadcasted_iota(jnp.int32, (SEQ, SEQ), 0)
    cols16 = lax.broadcasted_iota(jnp.int32, (SEQ, SEQ), 1)

    def rank_col(k):
        same = (ids_col[k] == ids_row[0]).astype(jnp.int32) + (ids_col[k] == ids_row[1]).astype(jnp.int32)
        return jnp.sum(jnp.where(cols16 < rows16, same, 0), axis=1, keepdims=True)

    def rank_row(k):
        same = (ids_row[k] == ids_col[0]).astype(jnp.int32) + (ids_row[k] == ids_col[1]).astype(jnp.int32)
        return jnp.sum(jnp.where(rows16 < cols16, same, 0), axis=0, keepdims=True)

    slot_row = lax.broadcasted_iota(jnp.int32, (EXPERTS * CAP, SEQ), 0)
    disp = jnp.zeros((EXPERTS * CAP, SEQ), F32)
    for k in range(2):
        disp = jnp.where(slot_row == ids_row[k] * CAP + rank_row(k), 1.0, disp)
    disp = disp.astype(BF)

    tab = table[...]
    chip = (((tab >> 4) + z) & 3) * 16 + ((((tab >> 2) & 3) + y) & 3) * 4 + (((tab & 3) + x) & 3)
    slot_lane = lax.broadcasted_iota(jnp.int32, (1, CHIPS * CAP), 1)
    slot_key = (chip >> 1) * CAP + (slot_lane & (CAP - 1))
    comb = jnp.zeros((SEQ, CHIPS * CAP), F32)
    for k in range(2):
        weight = jax.nn.sigmoid(logits[:, k : k + 1] - logits[:, 1 - k : 2 - k])
        comb = jnp.where(slot_key == ids_col[k] * CAP + rank_col(k), weight, comb)
    comb_hi = comb.astype(BF)
    comb_lo = (comb - comb_hi.astype(F32)).astype(BF)
    comb = jnp.concatenate([comb_hi, comb_lo], axis=0)

    residual = tokens[...].astype(F32)
    normed = rms(residual, mix_gain[...]).astype(BF)
    loads[0].wait()
    forget_pre = jnp.dot(normed, wf_v[...], preferred_element_type=F32)
    low = floor[...]
    forget = low + (1.0 - low) * jax.nn.sigmoid(forget_pre)
    key = (1.0 - low) * jax.nn.sigmoid(-forget_pre)
    loads[1].wait()
    query = jnp.dot(normed, wq_v[...], preferred_element_type=F32)
    query_forget = query * forget
    query_key = query * key
    loads[2].wait()
    value = jnp.dot(normed, wi_v[...], preferred_element_type=F32)
    value_out[...] = value
    for h in range(HEADS):
        lanes = slice(h * HEAD, (h + 1) * HEAD)
        forget_t[h] = forget[:, lanes].T
    for copy in prev_loads:
        copy.wait()
    expert_loads = [
        pltpu.make_async_copy(src.at[0], dst, expert_sem.at[i])
        for i, (src, dst) in enumerate(((w_gate, eg_v), (w_up, eu_v), (w_down, ed_v)))
    ]
    for copy in expert_loads:
        copy.start()
    for h in range(HEADS):
        lanes = slice(h * HEAD, (h + 1) * HEAD)
        columns = query_forget[:, lanes].T
        for s in range(SEQ):
            readout_v[s : s + 1, lanes] = jnp.sum(columns[:, s : s + 1] * prev_v[s, h], axis=0, keepdims=True)
    loads[3].wait()
    outgate_pre = jnp.dot(normed, wg_v[...], preferred_element_type=F32)
    gate = outgate_pre * jax.nn.sigmoid(outgate_pre)
    gated = []
    for h in range(HEADS):
        lanes = slice(h * HEAD, (h + 1) * HEAD)
        dotted = jnp.sum(query_key[:, lanes], axis=1, keepdims=True)
        readout = readout_v[:, lanes] + dotted * value[:, lanes]
        gated.append((rms(readout, head_gain[...]) * gate[:, lanes]).astype(BF))
    gated = jnp.concatenate(gated, axis=1)
    loads[4].wait()
    part_own[...] = jnp.dot(gated, wo_v[...], preferred_element_type=F32).astype(BF)

    pl.semaphore_wait(barrier, CHIPS)
    swap = to_sibling(part_own, part_sib, pair_sem.at[0], pair_sem.at[1])
    swap.start()
    swap.wait()
    middle = (residual + (part_own[...].astype(F32) + part_sib[...].astype(F32))).astype(BF)
    middle_v[...] = middle
    n2_v[...] = rms(middle.astype(F32), moe_gain[...]).astype(BF)
    mine = pl.ds(pl.multiple_of(c * HALF, HALF), HALF)
    theirs = pl.ds(pl.multiple_of(other * HALF, HALF), HALF)
    rows = jnp.dot(disp, n2_v[:, mine], preferred_element_type=F32)
    outgoing[...] = rows.reshape(EXPERTS, CAP, HALF).astype(BF)

    def slots(ref, k, first=0):
        return ref.at[pl.ds(k * PER + first, PER - first)]

    def wait_for(ref, k, sem):
        first = 1 if k == 0 else 0
        pltpu.make_async_copy(slots(ref, k, first), slots(ref, k, first), sem).wait()

    for i, o in enumerate(OFFSETS):
        if i == 0:
            continue
        to = ahead(o)
        pltpu.make_async_remote_copy(
            src_ref=outgoing.at[lax.div(to, 2)],
            dst_ref=inbox.at[c, i],
            send_sem=disp_send.at[i // PER],
            recv_sem=disp_recv.at[i // PER],
            device_id={"ep": to},
            device_id_type=MESH,
        ).start()
    inbox[c, 0] = outgoing[lax.div(me, 2)]

    def flat(values):
        return values.astype(F32).reshape(ROWS, HALF).astype(BF)

    def finish(k):
        down_swaps[k].wait()
        total = own_down[k] + down_recv[k].astype(F32)
        ret_out[pl.ds(k * PER, PER)] = total.reshape(PER, CAP, HALF).astype(BF)
        for j in range(PER):
            i = k * PER + j
            if i == 0:
                ret_in[0] = ret_out[0]
                continue
            pltpu.make_async_remote_copy(
                src_ref=ret_out.at[i],
                dst_ref=ret_in.at[i],
                send_sem=ret_send.at[k],
                recv_sem=ret_recv.at[k],
                device_id={"ep": behind(OFFSETS[i])},
                device_id_type=MESH,
            ).start()

    down_swaps, own_down = [], []
    for k in range(CHUNKS):
        wait_for(inbox.at[c], k, disp_recv.at[k])
        forward = to_sibling(slots(inbox.at[c], k), slots(inbox.at[c], k), fwd_send.at[k], fwd_recv.at[k])
        forward.start()
        if k == 0:
            for copy in expert_loads:
                copy.wait()
        rows = flat(inbox[c, pl.ds(k * PER, PER)])
        gate_pre = jnp.dot(rows, eg_v[mine, :], preferred_element_type=F32)
        up_pre = jnp.dot(rows, eu_v[mine, :], preferred_element_type=F32)
        if k > 0:
            finish(k - 1)
        forward.wait()
        rows = flat(inbox[other, pl.ds(k * PER, PER)])
        gate_pre = gate_pre + jnp.dot(rows, eg_v[theirs, :], preferred_element_type=F32)
        up_pre = up_pre + jnp.dot(rows, eu_v[theirs, :], preferred_element_type=F32)
        activated = (gate_pre * jax.nn.sigmoid(gate_pre) * up_pre).astype(BF)
        down_send[k] = jnp.dot(activated, ed_v[:, theirs], preferred_element_type=F32).astype(BF)
        swap = to_sibling(down_send.at[k], down_recv.at[k], down_sems.at[k], down_recv_sems.at[k])
        swap.start()
        down_swaps.append(swap)
        own_down.append(jnp.dot(activated, ed_v[:, mine], preferred_element_type=F32))
    finish(CHUNKS - 1)

    total = jnp.zeros((2 * SEQ, HALF), F32)
    for k in range(CHUNKS):
        wait_for(ret_in, k, ret_recv.at[k])
        total += jnp.dot(
            comb[:, k * ROWS : (k + 1) * ROWS], flat(ret_in[pl.ds(k * PER, PER)]), preferred_element_type=F32
        )
    expert_sum = total[:SEQ] + total[SEQ:]
    final[c] = (middle_v[:, mine].astype(F32) + expert_sum).astype(BF)
    swap = to_sibling(final.at[c], final.at[c], pair_sem.at[2], pair_sem.at[3])
    swap.start()
    swap.wait()
    out[:, :HALF] = final[0]
    out[:, HALF:] = final[1]
    for k in range(CHUNKS):
        wait_for(inbox.at[c], k, disp_send.at[k])
        wait_for(ret_in, k, ret_send.at[k])


def state_kernel(forget_t, value, prev, new):
    for s in range(SEQ):
        vector = value[s : s + 1, :]
        new[s, 0] = vector + forget_t[0, :, s : s + 1] * (prev[s, 0] - vector)


def on_device(
    tokens,
    mix_gain,
    w_query,
    w_forget,
    w_input,
    w_outgate,
    decay_floor,
    head_gain,
    prev_state,
    w_output,
    moe_gain,
    route_ids,
    route_logits,
    w_exp_gate,
    w_exp_up,
    w_exp_down,
):
    vmem = pl.BlockSpec(memory_space=pltpu.VMEM)
    hbm = pl.BlockSpec(memory_space=pl.ANY)
    dma = pltpu.SemaphoreType.DMA
    layer_out, forget_t, value = pl.pallas_call(
        layer_kernel,
        name="layer",
        out_shape=(
            jax.ShapeDtypeStruct((SEQ, WIDTH), BF),
            jax.ShapeDtypeStruct((HEADS, HEAD, SEQ), F32),
            jax.ShapeDtypeStruct((SEQ, MIX), F32),
        ),
        in_specs=[vmem] * 9 + [hbm] * 9,
        out_specs=(vmem,) * 3,
        scratch_shapes=[
            pltpu.VMEM((WIDTH, MIX), BF),
            pltpu.VMEM((WIDTH, MIX), BF),
            pltpu.VMEM((WIDTH, MIX), BF),
            pltpu.VMEM((WIDTH, MIX), BF),
            pltpu.VMEM((SEQ, HEADS, HEAD, HEAD), F32),
            pltpu.VMEM((MIX, WIDTH), BF),
            pltpu.VMEM((WIDTH, HID), BF),
            pltpu.VMEM((WIDTH, HID), BF),
            pltpu.VMEM((HID, WIDTH), BF),
            pltpu.VMEM((SEQ, MIX), F32),
            pltpu.VMEM((SEQ, WIDTH), BF),
            pltpu.VMEM((SEQ, WIDTH), BF),
            pltpu.VMEM((SEQ, WIDTH), BF),
            pltpu.VMEM((SEQ, WIDTH), BF),
            pltpu.VMEM((EXPERTS, CAP, HALF), BF),
            pltpu.VMEM((2, CHIPS, CAP, HALF), BF),
            pltpu.VMEM((CHUNKS, ROWS, HALF), BF),
            pltpu.VMEM((CHUNKS, ROWS, HALF), BF),
            pltpu.VMEM((CHIPS, CAP, HALF), BF),
            pltpu.VMEM((CHIPS, CAP, HALF), BF),
            pltpu.VMEM((2, SEQ, HALF), BF),
            dma((5,)),
            dma((4,)),
            dma((3,)),
            dma((4,)),
            dma((CHUNKS,)),
            dma((CHUNKS,)),
            dma((CHUNKS,)),
            dma((CHUNKS,)),
            dma((CHUNKS,)),
            dma((CHUNKS,)),
            dma((CHUNKS,)),
            dma((CHUNKS,)),
        ],
        compiler_params=pltpu.CompilerParams(
            collective_id=0, has_side_effects=True, vmem_limit_bytes=60 * 1024 * 1024
        ),
    )(
        tokens,
        mix_gain[None, :],
        decay_floor[None, :],
        head_gain[None, :],
        moe_gain[None, :],
        route_ids,
        route_ids.T,
        route_logits,
        jnp.asarray(slot_table()),
        w_query,
        w_forget,
        w_input,
        w_outgate,
        prev_state,
        w_output,
        w_exp_gate,
        w_exp_up,
        w_exp_down,
    )
    by_head = pl.BlockSpec((SEQ, 1, HEAD, HEAD), lambda h: (0, h, 0, 0))
    new_state = pl.pallas_call(
        state_kernel,
        name="state",
        grid=(HEADS,),
        out_shape=jax.ShapeDtypeStruct((SEQ, HEADS, HEAD, HEAD), F32),
        in_specs=[
            pl.BlockSpec((1, HEAD, SEQ), lambda h: (h, 0, 0)),
            pl.BlockSpec((SEQ, HEAD), lambda h: (0, h)),
            by_head,
        ],
        out_specs=by_head,
        cost_estimate=pl.CostEstimate(flops=3 * SEQ * MIX * HEAD, bytes_accessed=8 * SEQ * MIX * HEAD, transcendentals=0),
    )(forget_t, value, prev_state)
    return (layer_out, new_state)


def solution(mesh):
    placed = (
        P("ep", None),
        P(),
        P(None, "tp"),
        P(None, "tp"),
        P(None, "tp"),
        P(None, "tp"),
        P("tp"),
        P(),
        P("ep", "tp", None, None),
        P("tp", None),
        P(),
        P("ep", None),
        P("ep", None),
        P("ep", None, "tp"),
        P("ep", None, "tp"),
        P("ep", "tp", None),
    )
    return jax.shard_map(
        on_device,
        mesh=mesh,
        in_specs=placed,
        out_specs=(P("ep", None), P("ep", "tp", None, None)),
        check_vma=False,
    )
```

time: 127 us -> 55.2 us (0.43)
  blocking collectives: 58.1 us -> 0 us
  Pallas kernels: 0 us -> 51 us
  matrix products: 22.1 us -> 0 us
  waiting for transfers between devices: 17.8 us -> 0 us
  other arithmetic: 13.4 us -> 0 us
  starting transfers between devices: 5.7 us -> 0 us
  local copies, waits for them, and re-layouts: 7.83 us -> 3.34 us
    all_to_all x3 -> x0, blocking collectives: 55.1 us -> none  [the longest x1 40.3 us: on_device(): lax.all_to_all(outgoing, 'ep', split_axis=0, concat_axis=0, tiled=True)]
    pallas_call x0 -> x2, Pallas kernels: none -> 51 us  [the longest x1 45.5 us: on_device(): pl.pallas_call(layer_kernel, name='layer', out_shape=(jax.ShapeDtypeStruc...]
    dot_general x8 -> x0, matrix products: 22.1 us -> none  [the longest x1 8.23 us: on_device(): jnp.dot(activated, w_exp_down[0], preferred_element_type=jnp.float32)]
    all_to_all x1 -> x0, waiting for transfers between devices: 17.8 us -> none  [on_device(): lax.all_to_all(answer, 'ep', split_axis=0, concat_axis=0, tiled=True)]
    reduce_sum x8 -> x0, other arithmetic: 13.1 us -> none  [the longest x1 8.11 us: on_device(): readout = jnp.sum(query_part[..., None] * new_state, axis=2)]
    all_to_all x1 -> x0, starting transfers between devices: 5.7 us -> none  [on_device(): lax.all_to_all(answer, 'ep', split_axis=0, concat_axis=0, tiled=True)]
    all_gather x1 -> x0, blocking collectives: 2.92 us -> none  [total_of_pieces(): return lax.all_gather(shard, axis).astype(jnp.float32).sum(0)]
    transpose x1 -> x0, local copies, waits for them, and re-layouts: 2.16 us -> none  [joined_along(): return jnp.moveaxis(pieces, 0, dim).reshape(shape)]
  transfers between devices with their start and end apart: 1 -> 0, of which waited for: 1 -> 0; matrix products, arithmetic and copies ran while one was open for 0% -> 0% of each run, Pallas kernels for 0% -> 0%
where the time goes in v1:
time: 55.2 us; the launch traced here: 55 us
  Pallas kernels  51 us (92%)
  local copies, waits for them, and re-layouts  3.34 us (6%)
  between operations  0.65 us (1%)
    pallas_call x1, Pallas kernels, on_device(): pl.pallas_call(layer_kernel, name='layer', out_shape=(jax.ShapeDtypeStruc...  45.5 us
    pallas_call x1, Pallas kernels, on_device(): pl.pallas_call(state_kernel, name='state', grid=(HEADS,), out_shape=jax.S...  5.46 us
    unnamed x5, local copies, waits for them, and re-layouts  3.34 us

profile of v1, /device:TPU:1, one launch (start us, length us, event | category | flops | bytes accessed | tf_op | source)
XLA Modules:
  0.0 55.0 jit_solution(9655051505297067999)
XLA Ops:
  0.6 1.4 %copy.20.logits = f32[16,2]{1,0:T(8,128)} copy(f32[16,2]{0,1:T(2,128)} %param.29) | data formatting | bytes 256 | tf_op args[12]
  2.0 1.4 %copy.19.ids = s32[16,2]{1,0:T(8,128)} copy(s32[16,2]{0,1:T(2,128)} %param.28) | data formatting | bytes 256 | tf_op args[11]
  3.3 45.5 %layer.1 = (bf16[16,2048]{1,0:T(8,128)(2,1)}, f32[4,128,16]{2,1,0:T(8,128)}, f32[16,512]{1,0:T(8,128)}) custom-call(bf16[16,2048]{1,0:T(8,128)(2,1)} %tokens.1, f32[1,2048]{1,0:T(1,128)} %bitcast.5, f32[1,512]{1,0:T(1,128)} %bitcast.8, f32[1,128]{1,0:T(1,128)} %bitcast.9, f32[1,2048]{1,0:T(1,128)} %bitcast.6, s32[16,2]{1,0:T(8,128)} %copy.19.ids, ...), custom_call_target="tpu_custom_call" | custom-call | tf_op jit(solution)/shard_map/layer/pallas_call | solution.py:351
  48.9 0.0 copy-start
  48.9 5.5 %state.1 = f32[16,4,128,128]{3,2,1,0:T(8,128)} custom-call(f32[4,128,16]{2,1,0:T(8,128)} %get-tuple-element.6.forget_t, f32[16,512]{1,0:T(8,128)} %get-tuple-element.7.value, f32[16,4,128,128]{3,2,1,0:T(8,128)} %prev.3), custom_call_target="tpu_custom_call" | custom-call | flops 3145728 | bytes 8388608 | tf_op jit(solution)/shard_map/state/pallas_call | solution.py:420
  54.3 0.0 copy-done
  54.3 0.6 %copy.22 = bf16[16,2048]{1,0:T(8,128)(2,1)} copy(bf16[16,2048]{1,0:T(8,128)(2,1)S(1)} %copy-done) | data formatting | bytes 131072
Async XLA Ops:
  48.9 5.5 %copy-start = (bf16[16,2048]{1,0:T(8,128)(2,1)S(1)}, bf16[16,2048]{1,0:T(8,128)(2,1)}, u32[]{:S(2)}) copy-start(bf16[16,2048]{1,0:T(8,128)(2,1)} %get-tuple-element.10) | copy-start | bytes 196612

commit v2 on v1

--- a/solution.py
+++ b/solution.py
@@ -16,6 +16,7 @@
 CHUNKS = 4
 PER = CHIPS // CHUNKS
 ROWS = PER * CAP
+OWN = CHIPS - PER
 SEQ = 16
 WIDTH = 2048
 HALF = WIDTH // 2
@@ -34,10 +35,8 @@
 
 def offset_order():
     every = [(z, y, x) for z in range(SIDE) for y in range(SIDE) for x in range(SIDE)]
-    order = []
-    for k in range(CHUNKS):
-        mine = [o for o in every if sum(o) % SIDE == k]
-        order += sorted(mine, key=lambda o: (o != (0, 0, 0), -hops(o), o))
+    order = sorted(every[1:], key=lambda o: (-hops(o), sum(o) % SIDE, o))
+    order.insert(OWN, (0, 0, 0))
     return order
 
 
@@ -54,15 +53,14 @@
 
 
 def layer_kernel(
-    tokens,
-    mix_gain,
-    floor,
-    head_gain,
-    moe_gain,
-    ids,
-    ids_t,
-    logits,
-    table,
+    tokens_h,
+    mix_gain_h,
+    floor_h,
+    head_gain_h,
+    moe_gain_h,
+    ids_h,
+    logits_h,
+    table_h,
     w_query,
     w_forget,
     w_input,
@@ -73,8 +71,15 @@
     w_up,
     w_down,
     out,
-    forget_t,
-    value_out,
+    new_state,
+    tokens,
+    mix_gain,
+    floor,
+    head_gain,
+    moe_gain,
+    ids_t,
+    logits_t,
+    table,
     wq_v,
     wf_v,
     wi_v,
@@ -96,6 +101,7 @@
     ret_out,
     ret_in,
     final,
+    small_sem,
     load_sem,
     prev_sem,
     expert_sem,
@@ -130,9 +136,24 @@
 
     barrier = pltpu.get_barrier_semaphore()
     pl.semaphore_signal(barrier, inc=1, device_id={"tp": other}, device_id_type=MESH)
-    for o in OFFSETS[1:]:
+    for o in OFFSETS[:OWN] + OFFSETS[OWN + 1 :]:
         pl.semaphore_signal(barrier, inc=1, device_id={"ep": ahead(o)}, device_id_type=MESH)
 
+    small = [
+        pltpu.make_async_copy(src, dst, small_sem.at[i])
+        for i, (src, dst) in enumerate(
+            (
+                (tokens_h, tokens),
+                (mix_gain_h, mix_gain),
+                (floor_h, floor),
+                (head_gain_h, head_gain),
+                (moe_gain_h, moe_gain),
+                (ids_h, ids_t),
+                (logits_h, logits_t),
+                (table_h, table),
+            )
+        )
+    ]
     loads = [
         pltpu.make_async_copy(src, dst, load_sem.at[i])
         for i, (src, dst) in enumerate(
@@ -142,6 +163,8 @@
     prev_loads = [
         pltpu.make_async_copy(prev.at[pl.ds(4 * i, 4)], prev_v.at[pl.ds(4 * i, 4)], prev_sem.at[i]) for i in range(4)
     ]
+    for copy in small:
+        copy.start()
     loads[0].start()
     loads[1].start()
     loads[2].start()
@@ -149,11 +172,17 @@
         copy.start()
     loads[3].start()
     loads[4].start()
-
-    ids_col = [ids[:, k : k + 1] for k in range(2)]
-    ids_row = [ids_t[k : k + 1, :] for k in range(2)]
+    for copy in small:
+        copy.wait()
+
     rows16 = lax.broadcasted_iota(jnp.int32, (SEQ, SEQ), 0)
     cols16 = lax.broadcasted_iota(jnp.int32, (SEQ, SEQ), 1)
+
+    def column(row):
+        return jnp.sum(jnp.where(rows16 == cols16, row, jnp.zeros_like(row)), axis=1, keepdims=True)
+
+    ids_row = [ids_t[k : k + 1, :] for k in range(2)]
+    ids_col = [column(row) for row in ids_row]
 
     def rank_col(k):
         same = (ids_col[k] == ids_row[0]).astype(jnp.int32) + (ids_col[k] == ids_row[1]).astype(jnp.int32)
@@ -175,7 +204,7 @@
     slot_key = (chip >> 1) * CAP + (slot_lane & (CAP - 1))
     comb = jnp.zeros((SEQ, CHIPS * CAP), F32)
     for k in range(2):
-        weight = jax.nn.sigmoid(logits[:, k : k + 1] - logits[:, 1 - k : 2 - k])
+        weight = column(jax.nn.sigmoid(logits_t[k : k + 1, :] - logits_t[1 - k : 2 - k, :]))
         comb = jnp.where(slot_key == ids_col[k] * CAP + rank_col(k), weight, comb)
     comb_hi = comb.astype(BF)
     comb_lo = (comb - comb_hi.astype(F32)).astype(BF)
@@ -194,10 +223,6 @@
     query_key = query * key
     loads[2].wait()
     value = jnp.dot(normed, wi_v[...], preferred_element_type=F32)
-    value_out[...] = value
-    for h in range(HEADS):
-        lanes = slice(h * HEAD, (h + 1) * HEAD)
-        forget_t[h] = forget[:, lanes].T
     for copy in prev_loads:
         copy.wait()
     expert_loads = [
@@ -240,11 +265,11 @@
         return ref.at[pl.ds(k * PER + first, PER - first)]
 
     def wait_for(ref, k, sem):
-        first = 1 if k == 0 else 0
+        first = 1 if k == OWN // PER else 0
         pltpu.make_async_copy(slots(ref, k, first), slots(ref, k, first), sem).wait()
 
     for i, o in enumerate(OFFSETS):
-        if i == 0:
+        if i == OWN:
             continue
         to = ahead(o)
         pltpu.make_async_remote_copy(
@@ -255,7 +280,14 @@
             device_id={"ep": to},
             device_id_type=MESH,
         ).start()
-    inbox[c, 0] = outgoing[lax.div(me, 2)]
+    inbox[c, OWN] = outgoing[lax.div(me, 2)]
+
+    for h in range(HEADS):
+        lanes = slice(h * HEAD, (h + 1) * HEAD)
+        columns = forget[:, lanes].T
+        for s in range(SEQ):
+            vector = value[s : s + 1, lanes]
+            new_state[s, h] = vector + columns[:, s : s + 1] * (prev_v[s, h] - vector)
 
     def flat(values):
         return values.astype(F32).reshape(ROWS, HALF).astype(BF)
@@ -266,8 +298,8 @@
         ret_out[pl.ds(k * PER, PER)] = total.reshape(PER, CAP, HALF).astype(BF)
         for j in range(PER):
             i = k * PER + j
-            if i == 0:
-                ret_in[0] = ret_out[0]
+            if i == OWN:
+                ret_in[OWN] = ret_out[OWN]
                 continue
             pltpu.make_async_remote_copy(
                 src_ref=ret_out.at[i],
@@ -321,12 +353,6 @@
         wait_for(ret_in, k, ret_send.at[k])
 
 
-def state_kernel(forget_t, value, prev, new):
-    for s in range(SEQ):
-        vector = value[s : s + 1, :]
-        new[s, 0] = vector + forget_t[0, :, s : s + 1] * (prev[s, 0] - vector)
-
-
 def on_device(
     tokens,
     mix_gain,
@@ -346,19 +372,26 @@
     w_exp_down,
 ):
     vmem = pl.BlockSpec(memory_space=pltpu.VMEM)
-    hbm = pl.BlockSpec(memory_space=pl.ANY)
+    hbm = pl.BlockSpec(memory_space=pltpu.HBM)
     dma = pltpu.SemaphoreType.DMA
-    layer_out, forget_t, value = pl.pallas_call(
+    layer_out, new_state = pl.pallas_call(
         layer_kernel,
         name="layer",
         out_shape=(
-            jax.ShapeDtypeStruct((SEQ, WIDTH), BF),
-            jax.ShapeDtypeStruct((HEADS, HEAD, SEQ), F32),
-            jax.ShapeDtypeStruct((SEQ, MIX), F32),
+            pltpu.VMEM((SEQ, WIDTH), BF),
+            pltpu.VMEM((SEQ, HEADS, HEAD, HEAD), F32),
         ),
-        in_specs=[vmem] * 9 + [hbm] * 9,
-        out_specs=(vmem,) * 3,
+        in_specs=[hbm] * 17,
+        out_specs=(vmem,) * 2,
         scratch_shapes=[
+            pltpu.VMEM((SEQ, WIDTH), BF),
+            pltpu.VMEM((1, WIDTH), F32),
+            pltpu.VMEM((1, MIX), F32),
+            pltpu.VMEM((1, HEAD), F32),
+            pltpu.VMEM((1, WIDTH), F32),
+            pltpu.VMEM((2, SEQ), jnp.int32),
+            pltpu.VMEM((2, SEQ), F32),
+            pltpu.VMEM((1, CHIPS * CAP), jnp.int32),
             pltpu.VMEM((WIDTH, MIX), BF),
             pltpu.VMEM((WIDTH, MIX), BF),
             pltpu.VMEM((WIDTH, MIX), BF),
@@ -380,6 +413,7 @@
             pltpu.VMEM((CHIPS, CAP, HALF), BF),
             pltpu.VMEM((CHIPS, CAP, HALF), BF),
             pltpu.VMEM((2, SEQ, HALF), BF),
+            dma((8,)),
             dma((5,)),
             dma((4,)),
             dma((3,)),
@@ -394,7 +428,7 @@
             dma((CHUNKS,)),
         ],
         compiler_params=pltpu.CompilerParams(
-            collective_id=0, has_side_effects=True, vmem_limit_bytes=60 * 1024 * 1024
+            collective_id=0, has_side_effects=True, vmem_limit_bytes=62750720
         ),
     )(
         tokens,
@@ -402,9 +436,8 @@
         decay_floor[None, :],
         head_gain[None, :],
         moe_gain[None, :],
-        route_ids,
         route_ids.T,
-        route_logits,
+        route_logits.T,
         jnp.asarray(slot_table()),
         w_query,
         w_forget,
@@ -416,20 +449,6 @@
         w_exp_up,
         w_exp_down,
     )
-    by_head = pl.BlockSpec((SEQ, 1, HEAD, HEAD), lambda h: (0, h, 0, 0))
-    new_state = pl.pallas_call(
-        state_kernel,
-        name="state",
-        grid=(HEADS,),
-        out_shape=jax.ShapeDtypeStruct((SEQ, HEADS, HEAD, HEAD), F32),
-        in_specs=[
-            pl.BlockSpec((1, HEAD, SEQ), lambda h: (h, 0, 0)),
-            pl.BlockSpec((SEQ, HEAD), lambda h: (0, h)),
-            by_head,
-        ],
-        out_specs=by_head,
-        cost_estimate=pl.CostEstimate(flops=3 * SEQ * MIX * HEAD, bytes_accessed=8 * SEQ * MIX * HEAD, transcendentals=0),
-    )(forget_t, value, prev_state)
     return (layer_out, new_state)
 
 

time: 55.2 us -> 49.9 us (0.904)
  Pallas kernels: 51 us -> 46.5 us
  local copies, waits for them, and re-layouts: 3.34 us -> 2.64 us
    pallas_call x2 -> x1, Pallas kernels: 51 us -> 46.5 us  [on_device(): pl.pallas_call(layer_kernel, name='layer', out_shape=(pltpu.VMEM((SEQ, WI...]
    unnamed x5 -> x2, local copies, waits for them, and re-layouts: 3.34 us -> 2.64 us
where the time goes in v2:
time: 49.9 us; the launch traced here: 49.8 us
  Pallas kernels  46.5 us (93%)
  local copies, waits for them, and re-layouts  2.64 us (5%)
  between operations  0.65 us (1%)
    pallas_call x1, Pallas kernels, on_device(): pl.pallas_call(layer_kernel, name='layer', out_shape=(pltpu.VMEM((SEQ, WI...  46.5 us
    unnamed x2, local copies, waits for them, and re-layouts  2.64 us

profile of v2, /device:TPU:1, one launch (start us, length us, event | category | flops | bytes accessed | tf_op | source)
XLA Modules:
  0.0 49.8 jit_solution(669130085398209849)
XLA Ops:
  0.6 46.5 %layer.1 = (bf16[16,2048]{1,0:T(8,128)(2,1)S(1)}, f32[16,4,128,128]{3,2,1,0:T(8,128)S(1)}) custom-call(bf16[16,2048]{1,0:T(8,128)(2,1)} %tokens_h.1, f32[1,2048]{1,0:T(1,128)} %bitcast.6, f32[1,512]{1,0:T(1,128)} %bitcast.8, f32[1,128]{1,0:T(1,128)} %bitcast.11, f32[1,2048]{1,0:T(1,128)} %bitcast.7, s32[2,16]{1,0:T(2,128)} %bitcast.9, f32[2,16]{1,0:T(2,128)} %bitcast.10, ...), custom_call_target="tpu_custom_call" | custom-call | tf_op jit(solution)/shard_map/layer/pallas_call | solution.py:377
  47.2 0.6 %copy.21 = bf16[16,2048]{1,0:T(8,128)(2,1)} copy(bf16[16,2048]{1,0:T(8,128)(2,1)S(1)} %get-tuple-element.2) | data formatting | bytes 131072
  47.8 2.0 %copy.22 = f32[16,4,128,128]{3,2,1,0:T(8,128)} copy(f32[16,4,128,128]{3,2,1,0:T(8,128)S(1)} %get-tuple-element.3) | data formatting | bytes 8388608

commit v3 on v2

--- a/solution.py
+++ b/solution.py
@@ -13,10 +13,10 @@
 CHIPS = SIDE**3
 EXPERTS = CHIPS // 2
 CAP = 8
-CHUNKS = 4
-PER = CHIPS // CHUNKS
-ROWS = PER * CAP
-OWN = CHIPS - PER
+SIZES = (16, 16, 16, 16)
+STARTS = tuple(sum(SIZES[:k]) for k in range(len(SIZES)))
+CHUNKS = len(SIZES)
+OWN = STARTS[-1]
 SEQ = 16
 WIDTH = 2048
 HALF = WIDTH // 2
@@ -25,6 +25,7 @@
 MIX = HEADS * HEAD
 HID = 768
 EPS = 1e-6
+AHEAD = 6
 BF = jnp.bfloat16
 F32 = jnp.float32
 
@@ -35,7 +36,7 @@
 
 def offset_order():
     every = [(z, y, x) for z in range(SIDE) for y in range(SIDE) for x in range(SIDE)]
-    order = sorted(every[1:], key=lambda o: (-hops(o), sum(o) % SIDE, o))
+    order = sorted(every[1:], key=lambda o: ((sum(o) - 1) % SIDE, -hops(o), o))
     order.insert(OWN, (0, 0, 0))
     return order
 
@@ -50,6 +51,11 @@
 
 def rms(values, gains):
     return values * lax.rsqrt(jnp.mean(values * values, axis=-1, keepdims=True) + EPS) * gains
+
+
+def halves(src, dst):
+    size = src.shape[0] // 2
+    return [(src.at[pl.ds(i * size, size)], dst.at[pl.ds(i * size, size)]) for i in range(2)]
 
 
 def layer_kernel(
@@ -103,8 +109,6 @@
     final,
     small_sem,
     load_sem,
-    prev_sem,
-    expert_sem,
     pair_sem,
     disp_send,
     disp_recv,
@@ -154,24 +158,26 @@
             )
         )
     ]
-    loads = [
-        pltpu.make_async_copy(src, dst, load_sem.at[i])
-        for i, (src, dst) in enumerate(
-            ((w_forget, wf_v), (w_query, wq_v), (w_input, wi_v), (w_outgate, wg_v), (w_output, wo_v))
-        )
-    ]
-    prev_loads = [
-        pltpu.make_async_copy(prev.at[pl.ds(4 * i, 4)], prev_v.at[pl.ds(4 * i, 4)], prev_sem.at[i]) for i in range(4)
-    ]
+    parts = []
+    for src, dst in ((w_forget, wf_v), (w_query, wq_v)):
+        parts += halves(src, dst)
+    parts += [(prev.at[pl.ds(4 * i, 4)], prev_v.at[pl.ds(4 * i, 4)]) for i in range(4)]
+    for src, dst in ((w_input, wi_v), (w_outgate, wg_v), (w_output, wo_v)):
+        parts += halves(src, dst)
+    parts += [(w_gate.at[0], eg_v), (w_up.at[0], eu_v), (w_down.at[0], ed_v)]
+    loads = [pltpu.make_async_copy(src, dst, load_sem.at[i]) for i, (src, dst) in enumerate(parts)]
+    expert_loads = loads[14:]
+
+    def arrive(first, count):
+        for i in range(first, first + count):
+            loads[i].wait()
+            if i + AHEAD < len(loads):
+                loads[i + AHEAD].start()
+
     for copy in small:
         copy.start()
-    loads[0].start()
-    loads[1].start()
-    loads[2].start()
-    for copy in prev_loads:
+    for copy in loads[:AHEAD]:
         copy.start()
-    loads[3].start()
-    loads[4].start()
     for copy in small:
         copy.wait()
 
@@ -212,31 +218,25 @@
 
     residual = tokens[...].astype(F32)
     normed = rms(residual, mix_gain[...]).astype(BF)
-    loads[0].wait()
+    arrive(0, 2)
     forget_pre = jnp.dot(normed, wf_v[...], preferred_element_type=F32)
     low = floor[...]
     forget = low + (1.0 - low) * jax.nn.sigmoid(forget_pre)
     key = (1.0 - low) * jax.nn.sigmoid(-forget_pre)
-    loads[1].wait()
+    arrive(2, 2)
     query = jnp.dot(normed, wq_v[...], preferred_element_type=F32)
     query_forget = query * forget
     query_key = query * key
-    loads[2].wait()
+    columns = [query_forget[:, h * HEAD : (h + 1) * HEAD].T for h in range(HEADS)]
+    for part in range(4):
+        arrive(4 + part, 1)
+        for s in range(4 * part, 4 * part + 4):
+            for h in range(HEADS):
+                lanes = slice(h * HEAD, (h + 1) * HEAD)
+                readout_v[s : s + 1, lanes] = jnp.sum(columns[h][:, s : s + 1] * prev_v[s, h], axis=0, keepdims=True)
+    arrive(8, 2)
     value = jnp.dot(normed, wi_v[...], preferred_element_type=F32)
-    for copy in prev_loads:
-        copy.wait()
-    expert_loads = [
-        pltpu.make_async_copy(src.at[0], dst, expert_sem.at[i])
-        for i, (src, dst) in enumerate(((w_gate, eg_v), (w_up, eu_v), (w_down, ed_v)))
-    ]
-    for copy in expert_loads:
-        copy.start()
-    for h in range(HEADS):
-        lanes = slice(h * HEAD, (h + 1) * HEAD)
-        columns = query_forget[:, lanes].T
-        for s in range(SEQ):
-            readout_v[s : s + 1, lanes] = jnp.sum(columns[:, s : s + 1] * prev_v[s, h], axis=0, keepdims=True)
-    loads[3].wait()
+    arrive(10, 2)
     outgate_pre = jnp.dot(normed, wg_v[...], preferred_element_type=F32)
     gate = outgate_pre * jax.nn.sigmoid(outgate_pre)
     gated = []
@@ -246,7 +246,7 @@
         readout = readout_v[:, lanes] + dotted * value[:, lanes]
         gated.append((rms(readout, head_gain[...]) * gate[:, lanes]).astype(BF))
     gated = jnp.concatenate(gated, axis=1)
-    loads[4].wait()
+    arrive(12, 2)
     part_own[...] = jnp.dot(gated, wo_v[...], preferred_element_type=F32).astype(BF)
 
     pl.semaphore_wait(barrier, CHIPS)
@@ -262,10 +262,13 @@
     outgoing[...] = rows.reshape(EXPERTS, CAP, HALF).astype(BF)
 
     def slots(ref, k, first=0):
-        return ref.at[pl.ds(k * PER + first, PER - first)]
+        return ref.at[pl.ds(STARTS[k] + first, SIZES[k] - first)]
+
+    def chunk_of(i):
+        return max(k for k in range(CHUNKS) if STARTS[k] <= i)
 
     def wait_for(ref, k, sem):
-        first = 1 if k == OWN // PER else 0
+        first = 1 if k == chunk_of(OWN) else 0
         pltpu.make_async_copy(slots(ref, k, first), slots(ref, k, first), sem).wait()
 
     for i, o in enumerate(OFFSETS):
@@ -275,8 +278,8 @@
         pltpu.make_async_remote_copy(
             src_ref=outgoing.at[lax.div(to, 2)],
             dst_ref=inbox.at[c, i],
-            send_sem=disp_send.at[i // PER],
-            recv_sem=disp_recv.at[i // PER],
+            send_sem=disp_send.at[chunk_of(i)],
+            recv_sem=disp_recv.at[chunk_of(i)],
             device_id={"ep": to},
             device_id_type=MESH,
         ).start()
@@ -289,15 +292,17 @@
             vector = value[s : s + 1, lanes]
             new_state[s, h] = vector + columns[:, s : s + 1] * (prev_v[s, h] - vector)
 
+    def rows_of(k):
+        return pl.ds(STARTS[k] * CAP, SIZES[k] * CAP)
+
     def flat(values):
-        return values.astype(F32).reshape(ROWS, HALF).astype(BF)
+        return values.astype(F32).reshape(values.shape[0] * CAP, HALF).astype(BF)
 
     def finish(k):
         down_swaps[k].wait()
-        total = own_down[k] + down_recv[k].astype(F32)
-        ret_out[pl.ds(k * PER, PER)] = total.reshape(PER, CAP, HALF).astype(BF)
-        for j in range(PER):
-            i = k * PER + j
+        total = own_down[k] + down_recv[rows_of(k)].astype(F32)
+        ret_out[pl.ds(STARTS[k], SIZES[k])] = total.reshape(SIZES[k], CAP, HALF).astype(BF)
+        for i in range(STARTS[k], STARTS[k] + SIZES[k]):
             if i == OWN:
                 ret_in[OWN] = ret_out[OWN]
                 continue
@@ -318,18 +323,18 @@
         if k == 0:
             for copy in expert_loads:
                 copy.wait()
-        rows = flat(inbox[c, pl.ds(k * PER, PER)])
+        rows = flat(inbox[c, pl.ds(STARTS[k], SIZES[k])])
         gate_pre = jnp.dot(rows, eg_v[mine, :], preferred_element_type=F32)
         up_pre = jnp.dot(rows, eu_v[mine, :], preferred_element_type=F32)
         if k > 0:
             finish(k - 1)
         forward.wait()
-        rows = flat(inbox[other, pl.ds(k * PER, PER)])
+        rows = flat(inbox[other, pl.ds(STARTS[k], SIZES[k])])
         gate_pre = gate_pre + jnp.dot(rows, eg_v[theirs, :], preferred_element_type=F32)
         up_pre = up_pre + jnp.dot(rows, eu_v[theirs, :], preferred_element_type=F32)
         activated = (gate_pre * jax.nn.sigmoid(gate_pre) * up_pre).astype(BF)
-        down_send[k] = jnp.dot(activated, ed_v[:, theirs], preferred_element_type=F32).astype(BF)
-        swap = to_sibling(down_send.at[k], down_recv.at[k], down_sems.at[k], down_recv_sems.at[k])
+        down_send[rows_of(k)] = jnp.dot(activated, ed_v[:, theirs], preferred_element_type=F32).astype(BF)
+        swap = to_sibling(down_send.at[rows_of(k)], down_recv.at[rows_of(k)], down_sems.at[k], down_recv_sems.at[k])
         swap.start()
         down_swaps.append(swap)
         own_down.append(jnp.dot(activated, ed_v[:, mine], preferred_element_type=F32))
@@ -339,7 +344,9 @@
     for k in range(CHUNKS):
         wait_for(ret_in, k, ret_recv.at[k])
         total += jnp.dot(
-            comb[:, k * ROWS : (k + 1) * ROWS], flat(ret_in[pl.ds(k * PER, PER)]), preferred_element_type=F32
+            comb[:, STARTS[k] * CAP : (STARTS[k] + SIZES[k]) * CAP],
+            flat(ret_in[pl.ds(STARTS[k], SIZES[k])]),
+            preferred_element_type=F32,
         )
     expert_sum = total[:SEQ] + total[SEQ:]
     final[c] = (middle_v[:, mine].astype(F32) + expert_sum).astype(BF)
@@ -351,6 +358,17 @@
     for k in range(CHUNKS):
         wait_for(inbox.at[c], k, disp_send.at[k])
         wait_for(ret_in, k, ret_send.at[k])
+
+
+def deliver_kernel(made, state, out, new_state, sem):
+    copies = [pltpu.make_async_copy(made, out, sem.at[4])]
+    for i in range(4):
+        part = pl.ds(4 * i, 4)
+        copies.append(pltpu.make_async_copy(state.at[part], new_state.at[part], sem.at[i]))
+    for copy in copies:
+        copy.start()
+    for copy in copies:
+        copy.wait()
 
 
 def on_device(
@@ -408,15 +426,13 @@
             pltpu.VMEM((SEQ, WIDTH), BF),
             pltpu.VMEM((EXPERTS, CAP, HALF), BF),
             pltpu.VMEM((2, CHIPS, CAP, HALF), BF),
-            pltpu.VMEM((CHUNKS, ROWS, HALF), BF),
-            pltpu.VMEM((CHUNKS, ROWS, HALF), BF),
+            pltpu.VMEM((CHIPS * CAP, HALF), BF),
+            pltpu.VMEM((CHIPS * CAP, HALF), BF),
             pltpu.VMEM((CHIPS, CAP, HALF), BF),
             pltpu.VMEM((CHIPS, CAP, HALF), BF),
             pltpu.VMEM((2, SEQ, HALF), BF),
             dma((8,)),
-            dma((5,)),
-            dma((4,)),
-            dma((3,)),
+            dma((17,)),
             dma((4,)),
             dma((CHUNKS,)),
             dma((CHUNKS,)),
@@ -449,7 +465,18 @@
         w_exp_up,
         w_exp_down,
     )
-    return (layer_out, new_state)
+    return pl.pallas_call(
+        deliver_kernel,
+        name="deliver",
+        out_shape=(
+            jax.ShapeDtypeStruct((SEQ, WIDTH), BF),
+            jax.ShapeDtypeStruct((SEQ, HEADS, HEAD, HEAD), F32),
+        ),
+        in_specs=[vmem, vmem],
+        out_specs=(hbm, hbm),
+        scratch_shapes=[dma((5,))],
+        compiler_params=pltpu.CompilerParams(vmem_limit_bytes=6 * 1024 * 1024),
+    )(layer_out, new_state)
 
 
 def solution(mesh):

time: 49.9 us -> 47.2 us (0.946)
  local copies, waits for them, and re-layouts: 2.64 us -> 0 us
    unnamed x2 -> x0, local copies, waits for them, and re-layouts: 2.64 us -> none
    pallas_call x1, Pallas kernels: 46.5 us -> 44.4 us  [on_device(): pl.pallas_call(layer_kernel, name='layer', out_shape=(pltpu.VMEM((SEQ, WI...]
    pallas_call x0 -> x1, Pallas kernels: none -> 2.07 us  [on_device(): pl.pallas_call(deliver_kernel, name='deliver', out_shape=(jax.ShapeDtypeS...]
where the time goes in v3:
time: 47.2 us; the launch traced here: 47.1 us
  Pallas kernels  46.5 us (99%)
  between operations  0.64 us (1%)
    pallas_call x1, Pallas kernels, on_device(): pl.pallas_call(layer_kernel, name='layer', out_shape=(pltpu.VMEM((SEQ, WI...  44.4 us
    pallas_call x1, Pallas kernels, on_device(): pl.pallas_call(deliver_kernel, name='deliver', out_shape=(jax.ShapeDtypeS...  2.07 us

profile of v3, /device:TPU:1, one launch (start us, length us, event | category | flops | bytes accessed | tf_op | source)
XLA Modules:
  0.0 47.1 jit_solution(2658318268214865832)
XLA Ops:
  0.6 44.4 %layer.1 = (bf16[16,2048]{1,0:T(8,128)(2,1)S(1)}, f32[16,4,128,128]{3,2,1,0:T(8,128)S(1)}) custom-call(bf16[16,2048]{1,0:T(8,128)(2,1)} %tokens_h.1, f32[1,2048]{1,0:T(1,128)} %bitcast.6, f32[1,512]{1,0:T(1,128)} %bitcast.8, f32[1,128]{1,0:T(1,128)} %bitcast.11, f32[1,2048]{1,0:T(1,128)} %bitcast.7, s32[2,16]{1,0:T(2,128)} %bitcast.9, f32[2,16]{1,0:T(2,128)} %bitcast.10, ...), custom_call_target="tpu_custom_call" | custom-call | tf_op jit(solution)/shard_map/layer/pallas_call | solution.py:395
  45.0 2.1 %deliver.1 = (bf16[16,2048]{1,0:T(8,128)(2,1)}, f32[16,4,128,128]{3,2,1,0:T(8,128)}) custom-call(bf16[16,2048]{1,0:T(8,128)(2,1)S(1)} %get-tuple-element.4.made, f32[16,4,128,128]{3,2,1,0:T(8,128)S(1)} %get-tuple-element.5.state), custom_call_target="tpu_custom_call" | custom-call | tf_op jit(solution)/shard_map/deliver/pallas_call | solution.py:468

commit v4 on v3

--- a/solution.py
+++ b/solution.py
@@ -26,6 +26,7 @@
 HID = 768
 EPS = 1e-6
 AHEAD = 6
+MIX_LOADS = 14
 BF = jnp.bfloat16
 F32 = jnp.float32
 
@@ -36,7 +37,7 @@
 
 def offset_order():
     every = [(z, y, x) for z in range(SIDE) for y in range(SIDE) for x in range(SIDE)]
-    order = sorted(every[1:], key=lambda o: ((sum(o) - 1) % SIDE, -hops(o), o))
+    order = sorted(every[1:], key=lambda o: ((sum(o) - 1) % SIDE, -hops(o), min(o, tuple(-v % SIDE for v in o)), o))
     order.insert(OWN, (0, 0, 0))
     return order
 
@@ -166,12 +167,12 @@
         parts += halves(src, dst)
     parts += [(w_gate.at[0], eg_v), (w_up.at[0], eu_v), (w_down.at[0], ed_v)]
     loads = [pltpu.make_async_copy(src, dst, load_sem.at[i]) for i, (src, dst) in enumerate(parts)]
-    expert_loads = loads[14:]
+    expert_loads = loads[MIX_LOADS:]
 
     def arrive(first, count):
         for i in range(first, first + count):
             loads[i].wait()
-            if i + AHEAD < len(loads):
+            if i + AHEAD < MIX_LOADS:
                 loads[i + AHEAD].start()
 
     for copy in small:
@@ -181,6 +182,13 @@
     for copy in small:
         copy.wait()
 
+    residual = tokens[...].astype(F32)
+    normed = rms(residual, mix_gain[...]).astype(BF)
+    arrive(0, 2)
+    forget_pre = jnp.dot(normed, wf_v[...], preferred_element_type=F32)
+    low = floor[...]
+    forget = low + (1.0 - low) * jax.nn.sigmoid(forget_pre)
+    key = (1.0 - low) * jax.nn.sigmoid(-forget_pre)
     rows16 = lax.broadcasted_iota(jnp.int32, (SEQ, SEQ), 0)
     cols16 = lax.broadcasted_iota(jnp.int32, (SEQ, SEQ), 1)
 
@@ -216,13 +224,6 @@
     comb_lo = (comb - comb_hi.astype(F32)).astype(BF)
     comb = jnp.concatenate([comb_hi, comb_lo], axis=0)
 
-    residual = tokens[...].astype(F32)
-    normed = rms(residual, mix_gain[...]).astype(BF)
-    arrive(0, 2)
-    forget_pre = jnp.dot(normed, wf_v[...], preferred_element_type=F32)
-    low = floor[...]
-    forget = low + (1.0 - low) * jax.nn.sigmoid(forget_pre)
-    key = (1.0 - low) * jax.nn.sigmoid(-forget_pre)
     arrive(2, 2)
     query = jnp.dot(normed, wq_v[...], preferred_element_type=F32)
     query_forget = query * forget
@@ -247,6 +248,8 @@
         gated.append((rms(readout, head_gain[...]) * gate[:, lanes]).astype(BF))
     gated = jnp.concatenate(gated, axis=1)
     arrive(12, 2)
+    for copy in expert_loads:
+        copy.start()
     part_own[...] = jnp.dot(gated, wo_v[...], preferred_element_type=F32).astype(BF)
 
     pl.semaphore_wait(barrier, CHIPS)

time: 47.2 us -> 46.7 us (0.989)
  Pallas kernels: 46.5 us -> 45.9 us
    pallas_call x1, Pallas kernels: 44.4 us -> 43.8 us  [on_device(): pl.pallas_call(layer_kernel, name='layer', out_shape=(pltpu.VMEM((SEQ, WI...]
where the time goes in v4:
time: 46.7 us; the launch traced here: 46.6 us
  Pallas kernels  45.9 us (98%)
  between operations  0.64 us (1%)
    pallas_call x1, Pallas kernels, on_device(): pl.pallas_call(layer_kernel, name='layer', out_shape=(pltpu.VMEM((SEQ, WI...  43.8 us
    pallas_call x1, Pallas kernels, on_device(): pl.pallas_call(deliver_kernel, name='deliver', out_shape=(jax.ShapeDtypeS...  2.07 us

profile of v4, /device:TPU:1, one launch (start us, length us, event | category | flops | bytes accessed | tf_op | source)
XLA Modules:
  0.0 46.6 jit_solution(10350762610003225888)
XLA Ops:
  0.6 43.8 %layer.1 = (bf16[16,2048]{1,0:T(8,128)(2,1)S(1)}, f32[16,4,128,128]{3,2,1,0:T(8,128)S(1)}) custom-call(bf16[16,2048]{1,0:T(8,128)(2,1)} %tokens_h.1, f32[1,2048]{1,0:T(1,128)} %bitcast.6, f32[1,512]{1,0:T(1,128)} %bitcast.8, f32[1,128]{1,0:T(1,128)} %bitcast.11, f32[1,2048]{1,0:T(1,128)} %bitcast.7, s32[2,16]{1,0:T(2,128)} %bitcast.9, f32[2,16]{1,0:T(2,128)} %bitcast.10, ...), custom_call_target="tpu_custom_call" | custom-call | tf_op jit(solution)/shard_map/layer/pallas_call | solution.py:398
  44.5 2.1 %deliver.1 = (bf16[16,2048]{1,0:T(8,128)(2,1)}, f32[16,4,128,128]{3,2,1,0:T(8,128)}) custom-call(bf16[16,2048]{1,0:T(8,128)(2,1)S(1)} %get-tuple-element.4.made, f32[16,4,128,128]{3,2,1,0:T(8,128)S(1)} %get-tuple-element.5.state), custom_call_target="tpu_custom_call" | custom-call | tf_op jit(solution)/shard_map/deliver/pallas_call | solution.py:471
